TPU v7x, 32 devices: a whole 2x2x4 slice. The times are simulated.
32 devices in a mesh: sp: 8 (over z, y), tp: 4 (over x, core).
Axes of the slice: x: 2, y: 2, z: 4, core: 2. Of those that a mesh axis runs over, the one named last changes fastest.
Arguments:
- queries: bfloat16 [2304, 2048], P('sp', 'tp'), as said below
- key_vectors: bfloat16 [2304, 2048], P('sp', 'tp'), as said below
- latents: bfloat16 [2304, 2048], P('sp'), as said below
- value_weight: bfloat16 [2048, 2048], P(None, 'tp'), as said below
- log_sums: float32 [2304, 32], P('sp', 'tp'), as said below
- out_first: bfloat16 [2304, 2048], P('sp', 'tp'), as said below
- out_second: bfloat16 [2304, 2048], P('sp', 'tp'), as said below
- cotangent: bfloat16 [2304, 2048], P('sp', 'tp'), may hold values from -6 to 6
- head_lambda: float32 [16], P('tp'), may hold values from 0.3 to 0.8
Outputs:
- grad_queries: float32 [2304, 2048], P('sp', 'tp')
- grad_keys: float32 [2304, 2048], P('sp', 'tp')
- grad_latents: bfloat16 [2304, 2048], P('sp', 'tp')
- grad_weight: float32 [2048, 2048], P('sp', 'tp')
Inputs may be any that keep to these rules, and one draw needn't show every extreme that they name: queries with entries of standard deviation 1.75. `key_vectors`: keys with entries of standard deviation 1. `latents`: inputs of standard deviation 1. `value_weight`: weights scaled by the inverse square root of 2048. `log_sums`: each row's log-sum of exponentials of its causal scores, for the given queries and keys. `out_first`: the first map's attention output for the given queries, keys, values and log-sums. `out_second`: the second map's attention output, likewise.
All inputs are finite; a program needn't handle non-finite values.
Results may differ from a plain program's by a relative error of at most 0.022.
Values may be sent and summed in bfloat16 or wider, within the bound.
A program may use at most 192 MiB of HBM per device.

v0:
```python
import jax
import jax.numpy as jnp
from jax import lax
from jax.sharding import PartitionSpec as P

DH = 64
DV = 128


def row_terms(out_first, out_second, cotangent, head_lambda):
    count = out_first.shape[0]
    head_count = head_lambda.shape[0]
    first = out_first.astype(jnp.float32).reshape(count, head_count, DV)
    second = out_second.astype(jnp.float32).reshape(count, head_count, DV)
    mixed = first - head_lambda[None, :, None] * second
    inverse = lax.rsqrt(jnp.mean(mixed * mixed, axis=-1, keepdims=True) + 1e-06)
    normed = mixed * inverse
    grad_out = cotangent.astype(jnp.float32).reshape(count, head_count, DV)
    grad_mixed = inverse * (grad_out - normed * jnp.mean(grad_out * normed, axis=-1, keepdims=True))
    grad_rows = grad_mixed.astype(jnp.bfloat16)
    widened = lax.optimization_barrier(grad_rows).astype(jnp.float32)
    row_dots = jnp.stack(
        [jnp.sum(widened * first, axis=-1), jnp.sum(widened * second, axis=-1)], axis=-1
    )
    return (grad_rows.reshape(count, head_count * DV), row_dots.reshape(count, head_count * 2))


def block_grads(
    query_rows, grad_rows, lse_rows, dot_rows, query_pos, key_rows, value_rows, key_pos, head_lambda
):
    count = query_rows.shape[0]
    width = key_rows.shape[0]
    head_count = head_lambda.shape[0]
    score_scale = DH ** (-0.5)
    query_heads = query_rows.reshape(count, head_count, 2, DH)
    key_heads = key_rows.reshape(width, head_count, 2, DH)
    grad_heads = grad_rows.reshape(count, head_count, DV)
    value_heads = value_rows.reshape(width, head_count, DV)
    scores = (
        jnp.einsum("nhad,mhad->hanm", query_heads, key_heads, preferred_element_type=jnp.float32)
        * score_scale
    )
    causal = query_pos[:, None] >= key_pos[None, :]
    shifts = lse_rows.reshape(count, head_count, 2).transpose(1, 2, 0)[..., None]
    probs = jnp.exp(jnp.where(causal, scores - shifts, -1e30))
    d_attn = jnp.einsum("nhe,mhe->hnm", grad_heads, value_heads, preferred_element_type=jnp.float32)
    dots = dot_rows.reshape(count, head_count, 2).transpose(1, 2, 0)[..., None]
    map_weight = jnp.stack([jnp.ones_like(head_lambda), -head_lambda], axis=1)[:, :, None, None]
    d_scores = (map_weight * probs * (d_attn[:, None] - dots)).astype(jnp.bfloat16)
    weights = (probs[:, 0] - head_lambda[:, None, None] * probs[:, 1]).astype(jnp.bfloat16)
    grad_q = (
        jnp.einsum("hanm,mhad->nhad", d_scores, key_heads, preferred_element_type=jnp.float32)
        * score_scale
    )
    grad_k = (
        jnp.einsum("hanm,nhad->mhad", d_scores, query_heads, preferred_element_type=jnp.float32)
        * score_scale
    )
    grad_v = jnp.einsum("hnm,nhe->mhe", weights, grad_heads, preferred_element_type=jnp.float32)
    return (grad_q.reshape(count, -1), grad_k.reshape(width, -1), grad_v.reshape(width, -1))


def per_device(
    queries,
    key_vectors,
    latents,
    value_weight,
    log_sums,
    out_first,
    out_second,
    cotangent,
    head_lambda,
):
    local_rows = queries.shape[0]
    offset = lax.axis_index("sp") * local_rows
    positions = offset + jnp.arange(local_rows, dtype=jnp.int32)
    last_row = offset + local_rows - 1
    values = jnp.dot(latents, value_weight, preferred_element_type=jnp.float32).astype(jnp.bfloat16)
    grad_rows, row_dots = row_terms(out_first, out_second, cotangent, head_lambda)
    gathered_stats = (
        lax.all_gather(log_sums, "sp", axis=0, tiled=True),
        lax.all_gather(row_dots, "sp", axis=0, tiled=True),
    )
    key_rows = lax.all_gather(key_vectors, "sp", axis=0, tiled=True)
    value_rows = lax.all_gather(values, "sp", axis=0, tiled=True)
    count = key_rows.shape[0]

    def compute(current):
        key_pos = jnp.arange(count, dtype=jnp.int32)
        grad_q, unused_k, unused_v = block_grads(
            queries,
            grad_rows,
            log_sums,
            row_dots,
            positions,
            key_rows,
            value_rows,
            key_pos,
            head_lambda,
        )
        return grad_q

    grad_queries = lax.cond(
        jnp.int32(0) <= last_row,
        compute,
        lambda current: current,
        jnp.zeros((local_rows, queries.shape[1]), jnp.float32),
    )
    start_totals = (
        jnp.zeros((local_rows, key_vectors.shape[1]), jnp.float32),
        jnp.zeros((local_rows, values.shape[1]), jnp.float32),
    )
    query_rows = lax.all_gather(queries, "sp", axis=0, tiled=True)
    grad_piece = lax.all_gather(grad_rows, "sp", axis=0, tiled=True)
    add_count = query_rows.shape[0]

    def compute(current):
        query_pos = jnp.arange(add_count, dtype=jnp.int32)
        lse_rows = gathered_stats[0]
        dot_rows = gathered_stats[1]
        unused_q, grad_k, grad_v = block_grads(
            query_rows,
            grad_piece,
            lse_rows,
            dot_rows,
            query_pos,
            key_vectors,
            values,
            positions,
            head_lambda,
        )
        return (grad_k, grad_v)

    grad_keys, grad_values = lax.cond(
        jnp.int32(0) + add_count - 1 >= offset, compute, lambda current: current, start_totals
    )
    values_grad = grad_values.astype(jnp.bfloat16)
    grad_weight = lax.psum_scatter(
        lax.dot_general(
            latents, values_grad, (((0,), (0,)), ((), ())), preferred_element_type=jnp.float32
        ).astype(jnp.bfloat16),
        "sp",
        scatter_dimension=0,
        tiled=True,
    ).astype(jnp.float32)
    latent_partial = lax.dot_general(
        values_grad, value_weight, (((1,), (1,)), ((), ())), preferred_element_type=jnp.float32
    )
    grad_latents = lax.psum_scatter(
        latent_partial.astype(jnp.bfloat16), "tp", scatter_dimension=1, tiled=True
    )
    return (grad_queries, grad_keys, grad_latents, grad_weight)


def solution(mesh):
    return jax.shard_map(
        per_device,
        mesh=mesh,
        in_specs=(
            P("sp", "tp"),
            P("sp", "tp"),
            P("sp", None),
            P(None, "tp"),
            P("sp", "tp"),
            P("sp", "tp"),
            P("sp", "tp"),
            P("sp", "tp"),
            P("tp"),
        ),
        out_specs=(P("sp", "tp"), P("sp", "tp"), P("sp", "tp"), P("sp", "tp")),
        check_vma=False,
    )
```

profile of v0, /device:TPU:0, one launch (start us, length us, event | category | flops | bytes accessed | tf_op | source)
XLA Modules:
  0.0 336.8 jit_solution(91147204040858790)
XLA Ops:
  7.2 0.9 broadcast_bitcast_fusion
  8.1 1.2 convert_bitcast_fusion.1
  9.3 1.6 multiply_reduce_fusion
  11.1 1.6 fusion.38
  13.5 1.3 mul.122.clone
  15.2 2.1 fusion.33
  18.1 2.8 convolution_convert_fusion.2
  21.6 1.5 fusion.37
  24.3 33.1 %all-gather.1 = f32[8,288,8]{1,2,0:T(8,128)S(1)} all-gather(f32[1,288,8]{1,2,0:T(8,128)S(1)} %reshape.93), channel_id=1, replica_groups=mesh['sp'=8,'tp'=4] {'sp'}, dimensions={0}, use_global_device_ids=true | all-gather | bytes 82944 | tf_op jit(solution)/shard_map/all_gather | solution.py:82
  57.5 31.1 %all-gather = f32[8,288,8]{1,2,0:T(8,128)S(1)} all-gather(f32[1,288,8]{1,2,0:T(8,128)S(1)} %bitcast.156), channel_id=1, replica_groups=mesh['sp'=8,'tp'=4] {'sp'}, dimensions={0}, use_global_device_ids=true | all-gather | bytes 82944 | tf_op jit(solution)/shard_map/all_gather | solution.py:81
  88.7 37.1 %all-gather.11.cloned.1.call-done = bf16[2304,512]{1,0:T(8,128)(2,1)} async-done(((bf16[288,512]{1,0:T(8,128)(2,1)}), bf16[2304,512]{1,0:T(8,128)(2,1)}) %all-gather.11.cloned.1.call-update) | async-done | bytes 2359312 | tf_op jit(solution)/shard_map/all_gather | solution.py:113
  125.8 47.3 %conditional.3 = (bf16[288,512]{1,0:T(8,128)(2,1)}, f32[288,512]{1,0:T(8,128)}) conditional(s32[]{:T(128)} %convert_element_type.67, () %tuple.26, (f32[4]{0:T(128)S(1)}, s32[288]{0:T(512)S(1)}, bf16[2304,512]{1,0:T(8,128)(2,1)}, bf16[288,512]{1,0:T(8,128)(2,1)}, f32[2304,8]{0,1:T(8,128)S(1)}, /*index=5*/bf16[2304,512]{1,0:T(8,128)(2,1)}, ...), branch_computations={%region_6.7_spmd, %region_7.8_spmd} | conditional | flops 2763988992 | bytes 116491648 | solution.py:134
  125.8 4.4 %copy.149 = bf16[2304,512]{0,1:T(8,128)(2,1)} copy(bf16[2304,512]{1,0:T(8,128)(2,1)} %get-tuple-element.162) | data formatting | bytes 4718592 | tf_op jit(solution)/shard_map
  130.2 1.3 iota_compare_fusion.1
  131.8 11.4 %select_exponential_fusion = f32[4,2,2304,288]{2,3,1,0:T(8,128)} fusion(bf16[2304,4,2,64]{0,3,2,1:T(8,128)(2,1)} %bitcast.143, bf16[288,4,2,64]{0,3,2,1:T(8,128)(2,1)S(1)} %bitcast.153, f32[4,2,2304]{2,1,0:T(2,128)S(1)} %bitcast.155, pred[2304,288]{0,1:T(8,128)(4,1)} %iota_compare_fusion.1), kind=kOutput, calls=%fused_computation.10 | convolution fusion | flops 695402496 | bytes 24625152 | tf_op jit(solution)/shard_map/cond/branch_1_fun/nhad,mhad->hanm/dot_general | solution.py:40
  143.2 5.5 %fusion.12 = f32[4,2304,288]{1,2,0:T(8,128)} fusion(bf16[2304,512]{1,0:T(8,128)(2,1)S(1)} %copy-done.3, bf16[288,512]{1,0:T(8,128)(2,1)S(1)} %copy-done.4), kind=kOutput, calls=%fused_computation.20 | convolution fusion | flops 679477248 | bytes 13271040 | tf_op jit(solution)/shard_map/cond/branch_1_fun/nhe,mhe->hnm/dot_general | solution.py:46
  149.0 13.0 %fusion.16 = f32[4,2,288,64]{2,3,1,0:T(8,128)S(1)} fusion(bf16[2304,4,2,64]{0,3,2,1:T(8,128)(2,1)} %bitcast.144, f32[4,2,2304,288]{2,3,1,0:T(8,128)} %select_exponential_fusion, f32[4,2,2304]{2,1,0:T(2,128)S(1)} %bitcast.154, f32[4,2304,288]{1,2,0:T(8,128)} %fusion.12, f32[4,2]{1,0:T(4,128)S(1)} %stack.17.clone), kind=kOutput, calls=%fused_computation.24 | convolution fusion | flops 700858368 | bytes 34873376 | tf_op jit(solution)/shard_map/cond/branch_1_fun/hanm,nhad->mhad/dot_general | solution.py:56
  162.0 1.1 copy.157
  163.0 9.4 %fusion.22 = bf16[4,36,8,128]{3,2,1,0:T(8,128)(2,1)S(1)} fusion(f32[4,2,2304,288]{2,3,1,0:T(8,128)} %select_exponential_fusion, f32[4]{0:T(128)S(1)} %get-tuple-element.44, bf16[2304,512]{1,0:T(8,128)(2,1)} %get-tuple-element.49), kind=kOutput, calls=%fused_computation.26 | convolution fusion | flops 687587328 | bytes 23887888 | tf_op jit(solution)/shard_map/cond/branch_1_fun/hnm,nhe->mhe/dot_general | solution.py:59
  173.2 4.0 %fusion.29 = bf16[2048,512]{0,1:T(8,128)(2,1)} fusion(bf16[288,512]{1,0:T(8,128)(2,1)} %get-tuple-element.59, bf16[288,2048]{1,0:T(8,128)(2,1)} %param.15), kind=kOutput, calls=%fused_computation.32 | convolution fusion | flops 605028352 | bytes 3571712 | tf_op jit(solution)/shard_map/dot_general | solution.py:139
  177.5 2.8 convolution_convert_fusion.1
  180.4 51.1 %all-gather.7.cloned.1.call-done = bf16[2304,512]{1,0:T(8,128)(2,1)} async-done(((bf16[288,512]{1,0:T(8,128)(2,1)}), bf16[2304,512]{1,0:T(8,128)(2,1)}) %all-gather.7.cloned.1.call-update) | async-done | bytes 2359312 | tf_op jit(solution)/shard_map/all_gather | solution.py:84
  231.4 29.7 %conditional.2 = (f32[288,512]{1,0:T(8,128)}) conditional(s32[]{:T(128)} %convert_element_type.60, () %tuple.24, (f32[4]{0:T(128)S(1)}, s32[288]{0:T(512)S(1)}, bf16[288,512]{1,0:T(8,128)(2,1)S(1)}, bf16[2304,512]{1,0:T(8,128)(2,1)}, f32[288,8]{0,1:T(8,128)S(1)}, /*index=5*/bf16[2304,512]{1,0:T(8,128)(2,1)}, bf16[288,4,128]{2,0,1:T(8,128)(2,1)S(1)}, ...), branch_computations={%region_4.0_spmd, %region_5.6_spmd} | conditional | flops 2076401664 | bytes 35003676 | solution.py:103
  231.4 7.3 %fusion = f32[4,288,2304]{2,1,0:T(8,128)} fusion(bf16[288,4,128]{2,0,1:T(8,128)(2,1)S(1)} %get-tuple-element.41, bf16[2304,512]{1,0:T(8,128)(2,1)} %get-tuple-element.42), kind=kOutput, calls=%fused_computation.2 | convolution fusion | flops 679477248 | bytes 13271040 | tf_op jit(solution)/shard_map/cond/branch_1_fun/nhe,mhe->hnm/dot_general | solution.py:46
  238.7 4.3 %copy.142 = bf16[2304,512]{0,1:T(8,128)(2,1)} copy(bf16[2304,512]{1,0:T(8,128)(2,1)} %get-tuple-element.155) | data formatting | bytes 4718592 | tf_op jit(solution)/shard_map
  243.0 1.3 iota_compare_fusion
  244.3 0.9 copy.141
  245.6 14.5 %convolution_multiply_fusion = f32[4,2,288,64]{2,3,1,0:T(8,128)S(1)} fusion(bf16[2304,4,2,64]{0,3,2,1:T(8,128)(2,1)} %bitcast.146, bf16[288,4,2,64]{0,3,2,1:T(8,128)(2,1)} %bitcast.152, f32[4,2,288]{2,1,0:T(2,128)S(1)} %bitcast.157, f32[4,288,2304]{2,1,0:T(8,128)} %fusion, f32[4,2,288]{2,1,0:T(2,128)S(1)} %bitcast.158, f32[4,2]{1,0:T(4,128)S(1)} %stack.15.clone, ...), kind=kOutput, calls=%fused_computation.5 | convolution fusion | flops 1396260864 | bytes 14542880 | tf_op jit(solution)/shard_map/cond/branch_1_fun/hanm,mhad->nhad/dot_general | solution.py:52
  260.0 1.1 copy.155
  261.1 41.2 %reduce-scatter.5.cloned.1.call-done = bf16[256,512]{0,1:T(8,128)(2,1)} async-done(((bf16[2048,512]{0,1:T(8,128)(2,1)}), bf16[256,512]{0,1:T(8,128)(2,1)}) %reduce-scatter.5.cloned.1.call-update) | async-done | bytes 262160 | tf_op jit(solution)/shard_map/reduce_scatter | solution.py:138
  302.3 1.9 copy.153
  304.2 25.8 %reduce-scatter.3.cloned.1.call-done = bf16[288,512]{1,0:T(8,128)(2,1)} async-done(((bf16[288,2048]{1,0:T(8,128)(2,1)}), bf16[288,512]{1,0:T(8,128)(2,1)}) %reduce-scatter.3.cloned.1.call-update) | async-done | bytes 294928 | tf_op jit(solution)/shard_map/reduce_scatter | solution.py:149
  (62 shorter events, 6.2 us)
Async XLA Ops:
  7.2 11.0 %copy-start = (bf16[2048,512]{1,0:T(8,128)(2,1)S(1)}, bf16[2048,512]{1,0:T(8,128)(2,1)}, u32[]{:S(2)}) copy-start(bf16[2048,512]{1,0:T(8,128)(2,1)} %param.16) | copy-start | bytes 6291460
  7.2 81.5 %all-gather.13.cloned.1.call-start = ((), (), s32[]{:S(2)}) async-start(), calls=%async_computation.5 | async-start | bytes 2654208 | tf_op jit(solution)/shard_map/all_gather | solution.py:114
  17.3 108.5 %all-gather.11.cloned.1.call-start = ((), (), s32[]{:S(2)}) async-start(), calls=%async_computation.4 | async-start | bytes 2654208 | tf_op jit(solution)/shard_map/all_gather | solution.py:113
  18.1 162.3 %all-gather.9.cloned.1.call-start = ((), (), s32[]{:S(2)}) async-start(), calls=%async_computation.3 | async-start | bytes 2654208 | tf_op jit(solution)/shard_map/all_gather | solution.py:85
  20.9 36.6 %copy-start.7 = (f32[288,8]{0,1:T(8,128)S(1)}, f32[288,8]{0,1:T(8,128)}, u32[]{:S(2)}) copy-start(f32[288,8]{0,1:T(8,128)} %param.17) | copy-start | bytes 27652
  20.9 104.9 %copy-start.9 = (f32[4]{0:T(128)S(1)}, f32[4]{0:T(128)}, u32[]{:S(2)}) copy-start(f32[4]{0:T(128)} %param.21) | copy-start | bytes 52
  20.9 210.5 %all-gather.7.cloned.1.call-start = ((), (), s32[]{:S(2)}) async-start(), calls=%async_computation.2 | async-start | bytes 2654208 | tf_op jit(solution)/shard_map/all_gather | solution.py:84
  21.5 280.8 %reduce-scatter.5.cloned.1.call-start = ((), (), s32[]{:S(2)}) async-start(), calls=%async_computation.7 | async-start | bytes 2359296 | tf_op jit(solution)/shard_map/reduce_scatter | solution.py:138
  23.1 0.7 copy-start.1
  125.8 5.6 %copy-start.5 = (bf16[288,512]{1,0:T(8,128)(2,1)S(1)}, bf16[288,512]{1,0:T(8,128)(2,1)}, u32[]{:S(2)}) copy-start(bf16[288,512]{1,0:T(8,128)(2,1)} %get-tuple-element.163) | copy-start | bytes 884740 | tf_op jit(solution)/shard_map/cond
  131.8 11.4 %copy-start.3 = (bf16[2304,512]{1,0:T(8,128)(2,1)S(1)}, bf16[2304,512]{1,0:T(8,128)(2,1)}, u32[]{:S(2)}) copy-start(bf16[2304,512]{1,0:T(8,128)(2,1)} %get-tuple-element.49) | copy-start | bytes 7077892 | tf_op jit(solution)/shard_map/cond
  131.8 11.4 %copy-start.4 = (bf16[288,512]{1,0:T(8,128)(2,1)S(1)}, bf16[288,512]{1,0:T(8,128)(2,1)}, u32[]{:S(2)}) copy-start(bf16[288,512]{1,0:T(8,128)(2,1)} %get-tuple-element.50) | copy-start | bytes 884740 | tf_op jit(solution)/shard_map/cond
  177.2 54.2 %copy-start.2 = (bf16[288,4,128]{2,0,1:T(8,128)(2,1)S(1)}, bf16[288,4,128]{2,0,1:T(8,128)(2,1)}, u32[]{:S(2)}) copy-start(bf16[288,4,128]{2,0,1:T(8,128)(2,1)} %copy-done.1) | copy-start | bytes 884740
  177.2 54.2 %copy-start.6 = (bf16[288,512]{1,0:T(8,128)(2,1)S(1)}, bf16[288,512]{1,0:T(8,128)(2,1)}, u32[]{:S(2)}) copy-start(bf16[288,512]{1,0:T(8,128)(2,1)} %param.13) | copy-start | bytes 884740
  177.2 54.2 %copy-start.8 = (f32[288,8]{0,1:T(8,128)S(1)}, f32[288,8]{0,1:T(8,128)}, u32[]{:S(2)}) copy-start(f32[288,8]{0,1:T(8,128)} %param.17) | copy-start | bytes 27652
  177.2 152.7 %reduce-scatter.3.cloned.1.call-start = ((), (), s32[]{:S(2)}) async-start(), calls=%async_computation.6 | async-start | bytes 1474560 | tf_op jit(solution)/shard_map/reduce_scatter | solution.py:149
Sparse Core Ops, SparseCore 0:
  17.4 55.7 all-gather.12
  75.4 50.4 all-gather.10
  128.6 50.3 all-gather.8
  181.0 50.3 all-gather.6
  234.8 67.4 reduce-scatter.4
  305.3 24.6 reduce-scatter.2
where the time goes:
time: 337 us
  waiting for transfers between devices  156 us (46%)
  matrix products  70.6 us (21%)
  blocking collectives  64.1 us (19%)
  local copies, waits for them, and re-layouts  19.6 us (6%)
  between operations  14.3 us (4%)
  other arithmetic  11.2 us (3%)
    all_gather x1, waiting for transfers between devices, per_device(): key_rows = lax.all_gather(key_vectors, 'sp', axis=0, tiled=True)  51.1 us
    reduce_scatter x1, waiting for transfers between devices, per_device(): lax.psum_scatter(lax.dot_general(latents, values_grad, (((0,), (0,)), (()...  41.2 us
    all_gather x1, waiting for transfers between devices, per_device(): query_rows = lax.all_gather(queries, 'sp', axis=0, tiled=True)  37.1 us
    all_gather x1, blocking collectives, per_device(): lax.all_gather(row_dots, 'sp', axis=0, tiled=True)  33.1 us
    all_gather x1, blocking collectives, per_device(): lax.all_gather(log_sums, 'sp', axis=0, tiled=True)  31.1 us
    reduce_scatter x1, waiting for transfers between devices, per_device(): lax.psum_scatter(latent_partial.astype(jnp.bfloat16), 'tp', scatter_dimen...  25.8 us
    dot_general x1, matrix products, block_grads(): jnp.einsum('hanm,mhad->nhad', d_scores, key_heads, preferred_element_type...  14.5 us
    dot_general x1, matrix products, block_grads(): jnp.einsum('hanm,nhad->mhad', d_scores, query_heads, preferred_element_ty...  13 us
  transfers between devices with their start and end apart: 6, of which 4 were waited for; matrix products, arithmetic and copies ran while one was open for 27% of the time, Pallas kernels for 0%

commit v1 on v0

--- a/solution.py
+++ b/solution.py
@@ -110,7 +110,12 @@
         jnp.zeros((local_rows, key_vectors.shape[1]), jnp.float32),
         jnp.zeros((local_rows, values.shape[1]), jnp.float32),
     )
-    query_rows = lax.all_gather(queries, "sp", axis=0, tiled=True)
+    ring = [queries]
+    for hop in range(7):
+        ring.append(lax.ppermute(ring[-1], "sp", [(dev, (dev + 1) % 8) for dev in range(8)]))
+    query_rows = jnp.roll(
+        jnp.concatenate(ring[::-1], axis=0), (lax.axis_index("sp") + 1) * ring[0].shape[0], axis=0
+    )
     grad_piece = lax.all_gather(grad_rows, "sp", axis=0, tiled=True)
     add_count = query_rows.shape[0]
 

time: 337 us -> 361 us (1.071)
  local copies, waits for them, and re-layouts: 19.6 us -> 31.1 us
  blocking collectives: 64.1 us -> 69.7 us
    ppermute x0 -> x7, waiting for transfers between devices: none -> 99.8 us  [per_device(): lax.ppermute(ring[-1], 'sp', [(dev, (dev + 1) % 8) for dev in range(8)])]
    all_gather x1, waiting for transfers between devices: 51.1 us -> 0.02 us  [per_device(): key_rows = lax.all_gather(key_vectors, 'sp', axis=0, tiled=True)]
    all_gather x1 -> x0, waiting for transfers between devices: 37.1 us -> none  [per_device(): query_rows = lax.all_gather(queries, 'sp', axis=0, tiled=True)]
    concatenate x0 -> x1, local copies, waits for them, and re-layouts: none -> 9.47 us  [per_device(): jnp.roll(jnp.concatenate(ring[::-1], axis=0), (lax.axis_index('sp') + 1)...]
    reduce_scatter x1, waiting for transfers between devices: 41.2 us -> 33 us  [per_device(): lax.psum_scatter(lax.dot_general(latents, values_grad, (((0,), (0,)), (()...]
    all_gather x1, blocking collectives: 33.1 us -> 38.2 us  [per_device(): lax.all_gather(row_dots, 'sp', axis=0, tiled=True)]
    dynamic_slice x0 -> x1, local copies, waits for them, and re-layouts: none -> 4.55 us  [per_device(): jnp.roll(jnp.concatenate(ring[::-1], axis=0), (lax.axis_index('sp') + 1)...]
    another operation x5 -> x4, local copies, waits for them, and re-layouts: 9.96 us -> 5.61 us
  transfers between devices with their start and end apart: 6 -> 12, of which waited for: 4 -> 8; matrix products, arithmetic and copies ran while one was open for 27% -> 29% of each run, Pallas kernels for 0% -> 0%
where the time goes in v1:
time: 361 us; the launch traced here: 360 us
  waiting for transfers between devices  159 us (44%)
  matrix products  70.7 us (20%)
  blocking collectives  69.7 us (19%)
  local copies, waits for them, and re-layouts  31.1 us (9%)
  between operations  14.1 us (4%)
  other arithmetic  11.2 us (3%)
    ppermute x7, waiting for transfers between devices, per_device(): lax.ppermute(ring[-1], 'sp', [(dev, (dev + 1) % 8) for dev in range(8)])  99.8 us
    all_gather x1, blocking collectives, per_device(): lax.all_gather(row_dots, 'sp', axis=0, tiled=True)  38.2 us
    reduce_scatter x1, waiting for transfers between devices, per_device(): lax.psum_scatter(lax.dot_general(latents, values_grad, (((0,), (0,)), (()...  33 us
    all_gather x1, blocking collectives, per_device(): lax.all_gather(log_sums, 'sp', axis=0, tiled=True)  31.5 us
    reduce_scatter x1, waiting for transfers between devices, per_device(): lax.psum_scatter(latent_partial.astype(jnp.bfloat16), 'tp', scatter_dimen...  25.7 us
    dot_general x1, matrix products, block_grads(): jnp.einsum('hanm,mhad->nhad', d_scores, key_heads, preferred_element_type...  14.7 us
    dot_general x2, matrix products, block_grads(): jnp.einsum('nhe,mhe->hnm', grad_heads, value_heads, preferred_element_typ...  12.9 us
    dot_general x1, matrix products, block_grads(): jnp.einsum('hanm,nhad->mhad', d_scores, query_heads, preferred_element_ty...  12.8 us
  transfers between devices with their start and end apart: 12, of which 8 were waited for; matrix products, arithmetic and copies ran while one was open for 29% of the time, Pallas kernels for 0%

profile of v1, /device:TPU:0, one launch (start us, length us, event | category | flops | bytes accessed | tf_op | source)
XLA Modules:
  0.0 359.6 jit_solution(4507687163738664604)
XLA Ops:
  9.3 1.6 multiply_reduce_fusion
  11.1 1.6 fusion.38
  15.2 2.1 fusion.33
  17.4 2.8 convolution_convert_fusion.2
  21.0 1.9 copy.154
  22.8 3.0 collective-permute-start
  25.8 17.6 %collective-permute-done = bf16[288,512]{0,1:T(8,128)(2,1)S(1)} collective-permute-done((bf16[288,512]{0,1:T(8,128)(2,1)}, bf16[288,512]{0,1:T(8,128)(2,1)S(1)}, u32[]{:S(2)}, u32[]{:S(2)}) %collective-permute-start) | collective-permute-done | bytes 294944 | tf_op jit(solution)/shard_map/ppermute | solution.py:115
  43.4 12.7 %collective-permute-done.1 = bf16[288,512]{0,1:T(8,128)(2,1)S(1)} collective-permute-done((bf16[288,512]{0,1:T(8,128)(2,1)S(1)}, bf16[288,512]{0,1:T(8,128)(2,1)S(1)}, u32[]{:S(2)}, u32[]{:S(2)}) %collective-permute-start.1) | collective-permute-done | bytes 294944 | tf_op jit(solution)/shard_map/ppermute | solution.py:115
  56.1 19.8 %collective-permute-done.2 = bf16[288,512]{0,1:T(8,128)(2,1)S(1)} collective-permute-done((bf16[288,512]{0,1:T(8,128)(2,1)S(1)}, bf16[288,512]{0,1:T(8,128)(2,1)S(1)}, u32[]{:S(2)}, u32[]{:S(2)}) %collective-permute-start.2) | collective-permute-done | bytes 294944 | tf_op jit(solution)/shard_map/ppermute | solution.py:115
  76.0 20.8 %collective-permute-done.3 = bf16[288,512]{0,1:T(8,128)(2,1)S(1)} collective-permute-done((bf16[288,512]{0,1:T(8,128)(2,1)S(1)}, bf16[288,512]{0,1:T(8,128)(2,1)S(1)}, u32[]{:S(2)}, u32[]{:S(2)}) %collective-permute-start.3) | collective-permute-done | bytes 294944 | tf_op jit(solution)/shard_map/ppermute | solution.py:115
  96.8 12.8 %collective-permute-done.4 = bf16[288,512]{0,1:T(8,128)(2,1)} collective-permute-done((bf16[288,512]{0,1:T(8,128)(2,1)S(1)}, bf16[288,512]{0,1:T(8,128)(2,1)}, u32[]{:S(2)}, u32[]{:S(2)}) %collective-permute-start.4) | collective-permute-done | bytes 294944 | tf_op jit(solution)/shard_map/ppermute | solution.py:115
  109.7 1.5 fusion.37
  112.2 16.0 %collective-permute-done.5 = bf16[288,512]{0,1:T(8,128)(2,1)} collective-permute-done((bf16[288,512]{0,1:T(8,128)(2,1)}, bf16[288,512]{0,1:T(8,128)(2,1)}, u32[]{:S(2)}, u32[]{:S(2)}) %collective-permute-start.5) | collective-permute-done | bytes 294944 | tf_op jit(solution)/shard_map/ppermute | solution.py:115
  128.4 38.2 %all-gather.1 = f32[8,288,8]{1,2,0:T(8,128)S(1)} all-gather(f32[1,288,8]{1,2,0:T(8,128)S(1)} %reshape.117), channel_id=1, replica_groups=mesh['sp'=8,'tp'=4] {'sp'}, dimensions={0}, use_global_device_ids=true | all-gather | bytes 82944 | tf_op jit(solution)/shard_map/all_gather | solution.py:82
  166.7 31.5 %all-gather = f32[8,288,8]{1,2,0:T(8,128)S(1)} all-gather(f32[1,288,8]{1,2,0:T(8,128)S(1)} %bitcast.156), channel_id=1, replica_groups=mesh['sp'=8,'tp'=4] {'sp'}, dimensions={0}, use_global_device_ids=true | all-gather | bytes 82944 | tf_op jit(solution)/shard_map/all_gather | solution.py:81
  198.5 9.5 %concatenate.6 = bf16[4608,512]{0,1:T(8,128)(2,1)} concatenate(bf16[288,512]{0,1:T(8,128)(2,1)S(1)} %collective-permute-done.6, bf16[288,512]{0,1:T(8,128)(2,1)} %collective-permute-done.5, bf16[288,512]{0,1:T(8,128)(2,1)} %collective-permute-done.4, bf16[288,512]{0,1:T(8,128)(2,1)} %copy-done.7, bf16[288,512]{0,1:T(8,128)(2,1)} %copy-done.6, bf16[288,512]{0,1:T(8,128)(2,1)} %copy-done.5, ...), dimensions={0} | concatenate | bytes 9437184 | tf_op jit(solution)/shard_map/jit(_roll_dynamic)/concatenate | solution.py:116
  208.0 47.2 %conditional.3 = (bf16[288,512]{1,0:T(8,128)(2,1)}, f32[288,512]{1,0:T(8,128)}) conditional(s32[]{:T(128)} %convert_element_type.76, () %tuple.36, (f32[4]{0:T(128)S(1)}, s32[288]{0:T(512)S(1)}, s32[]{:T(128)}, bf16[4608,512]{0,1:T(8,128)(2,1)}, bf16[288,512]{1,0:T(8,128)(2,1)S(1)}, /*index=5*/f32[2304,8]{0,1:T(8,128)S(1)}, ...), branch_computations={%region_6.7_spmd, %region_7.8_spmd} | conditional | flops 2763988992 | bytes 114132432 | solution.py:139
  208.0 4.5 %constant_dynamic-slice_fusion = bf16[2304,512]{0,1:T(8,128)(2,1)} fusion(bf16[4608,512]{0,1:T(8,128)(2,1)} %get-tuple-element.158, s32[]{:T(128)S(6)} %select_n.29), kind=kLoop, calls=%fused_computation.31 | loop fusion | bytes 4718596 | tf_op jit(solution)/shard_map/jit(_roll_dynamic)/dynamic_slice | solution.py:116
  212.6 1.3 iota_compare_fusion.1
  214.1 11.4 %select_exponential_fusion = f32[4,2,2304,288]{2,3,1,0:T(8,128)} fusion(bf16[2304,4,2,64]{0,3,2,1:T(8,128)(2,1)} %bitcast.143, bf16[288,4,2,64]{0,3,2,1:T(8,128)(2,1)S(1)} %bitcast.153, f32[4,2,2304]{2,1,0:T(2,128)S(1)} %bitcast.155, pred[2304,288]{0,1:T(8,128)(4,1)} %iota_compare_fusion.1), kind=kOutput, calls=%fused_computation.10 | convolution fusion | flops 695402496 | bytes 24625152 | tf_op jit(solution)/shard_map/cond/branch_1_fun/nhad,mhad->hanm/dot_general | solution.py:40
  225.6 5.5 %fusion.12 = f32[4,2304,288]{1,2,0:T(8,128)} fusion(bf16[2304,512]{1,0:T(8,128)(2,1)S(1)} %copy-done.3, bf16[288,512]{1,0:T(8,128)(2,1)S(1)} %get-tuple-element.163), kind=kOutput, calls=%fused_computation.20 | convolution fusion | flops 679477248 | bytes 13271040 | tf_op jit(solution)/shard_map/cond/branch_1_fun/nhe,mhe->hnm/dot_general | solution.py:46
  231.3 12.8 %fusion.16 = f32[4,2,288,64]{2,3,1,0:T(8,128)S(1)} fusion(bf16[2304,4,2,64]{0,3,2,1:T(8,128)(2,1)} %bitcast.144, f32[4,2,2304,288]{2,3,1,0:T(8,128)} %select_exponential_fusion, f32[4,2,2304]{2,1,0:T(2,128)S(1)} %bitcast.154, f32[4,2304,288]{1,2,0:T(8,128)} %fusion.12, f32[4,2]{1,0:T(4,128)S(1)} %stack.20.clone), kind=kOutput, calls=%fused_computation.24 | convolution fusion | flops 700858368 | bytes 34873376 | tf_op jit(solution)/shard_map/cond/branch_1_fun/hanm,nhad->mhad/dot_general | solution.py:56
  245.2 9.3 %fusion.22 = bf16[4,36,8,128]{3,2,1,0:T(8,128)(2,1)S(1)} fusion(f32[4,2,2304,288]{2,3,1,0:T(8,128)} %select_exponential_fusion, f32[4]{0:T(128)S(1)} %get-tuple-element.156, bf16[2304,512]{1,0:T(8,128)(2,1)} %get-tuple-element.162), kind=kOutput, calls=%fused_computation.26 | convolution fusion | flops 687587328 | bytes 23887888 | tf_op jit(solution)/shard_map/cond/branch_1_fun/hnm,nhe->mhe/dot_general | solution.py:59
  255.2 4.0 %fusion.29 = bf16[2048,512]{0,1:T(8,128)(2,1)} fusion(bf16[288,512]{1,0:T(8,128)(2,1)} %get-tuple-element.172, bf16[288,2048]{1,0:T(8,128)(2,1)} %param.15), kind=kOutput, calls=%fused_computation.33 | convolution fusion | flops 605028352 | bytes 3571712 | tf_op jit(solution)/shard_map/dot_general | solution.py:144
  259.5 2.8 convolution_convert_fusion.1
  262.4 30.1 %conditional.2 = (f32[288,512]{1,0:T(8,128)}) conditional(s32[]{:T(128)} %convert_element_type.69, () %tuple.34, (f32[4]{0:T(128)S(1)}, s32[288]{0:T(512)S(1)}, bf16[288,512]{1,0:T(8,128)(2,1)S(1)}, bf16[2304,512]{1,0:T(8,128)(2,1)}, f32[288,8]{0,1:T(8,128)S(1)}, /*index=5*/bf16[2304,512]{1,0:T(8,128)(2,1)}, bf16[288,4,128]{2,0,1:T(8,128)(2,1)S(1)}, ...), branch_computations={%region_4.0_spmd, %region_5.6_spmd} | conditional | flops 2076401664 | bytes 35003676 | solution.py:103
  262.5 7.4 %fusion = f32[4,288,2304]{2,1,0:T(8,128)} fusion(bf16[288,4,128]{2,0,1:T(8,128)(2,1)S(1)} %get-tuple-element.153, bf16[2304,512]{1,0:T(8,128)(2,1)} %get-tuple-element.154), kind=kOutput, calls=%fused_computation.2 | convolution fusion | flops 679477248 | bytes 13271040 | tf_op jit(solution)/shard_map/cond/branch_1_fun/nhe,mhe->hnm/dot_general | solution.py:46
  269.8 4.3 %copy.152 = bf16[2304,512]{0,1:T(8,128)(2,1)} copy(bf16[2304,512]{1,0:T(8,128)(2,1)} %get-tuple-element.273) | data formatting | bytes 4718592 | tf_op jit(solution)/shard_map
  276.7 14.7 %convolution_multiply_fusion = f32[4,2,288,64]{2,3,1,0:T(8,128)S(1)} fusion(bf16[2304,4,2,64]{0,3,2,1:T(8,128)(2,1)} %bitcast.146, bf16[288,4,2,64]{0,3,2,1:T(8,128)(2,1)} %bitcast.152, f32[4,2,288]{2,1,0:T(2,128)S(1)} %bitcast.157, f32[4,288,2304]{2,1,0:T(8,128)} %fusion, f32[4,2,288]{2,1,0:T(2,128)S(1)} %bitcast.158, f32[4,2]{1,0:T(4,128)S(1)} %stack.18.clone, ...), kind=kOutput, calls=%fused_computation.5 | convolution fusion | flops 1396260864 | bytes 14542880 | tf_op jit(solution)/shard_map/cond/branch_1_fun/hanm,mhad->nhad/dot_general | solution.py:52
  292.5 33.0 %reduce-scatter.5.cloned.1.call-done = bf16[256,512]{0,1:T(8,128)(2,1)} async-done(((bf16[2048,512]{0,1:T(8,128)(2,1)}), bf16[256,512]{0,1:T(8,128)(2,1)}) %reduce-scatter.5.cloned.1.call-update) | async-done | bytes 262160 | tf_op jit(solution)/shard_map/reduce_scatter | solution.py:143
  325.5 1.9 copy.165
  327.4 25.7 %reduce-scatter.3.cloned.1.call-done = bf16[288,512]{1,0:T(8,128)(2,1)} async-done(((bf16[288,2048]{1,0:T(8,128)(2,1)}), bf16[288,512]{1,0:T(8,128)(2,1)}) %reduce-scatter.3.cloned.1.call-update) | async-done | bytes 294928 | tf_op jit(solution)/shard_map/reduce_scatter | solution.py:154
  (83 shorter events, 13.3 us)
Async XLA Ops:
  7.2 10.2 %copy-start = (bf16[2048,512]{1,0:T(8,128)(2,1)S(1)}, bf16[2048,512]{1,0:T(8,128)(2,1)}, u32[]{:S(2)}) copy-start(bf16[2048,512]{1,0:T(8,128)(2,1)} %param.16) | copy-start | bytes 6291460
  7.2 200.8 %all-gather.10.cloned.1.call-start = ((), (), s32[]{:S(2)}) async-start(), calls=%async_computation.4 | async-start | bytes 2654208 | tf_op jit(solution)/shard_map/all_gather | solution.py:119
  17.3 245.1 %all-gather.8.cloned.1.call-start = ((), (), s32[]{:S(2)}) async-start(), calls=%async_computation.3 | async-start | bytes 2654208 | tf_op jit(solution)/shard_map/all_gather | solution.py:85
  20.2 146.6 %copy-start.11 = (f32[288,8]{0,1:T(8,128)S(1)}, f32[288,8]{0,1:T(8,128)}, u32[]{:S(2)}) copy-start(f32[288,8]{0,1:T(8,128)} %param.17) | copy-start | bytes 27652
  20.2 242.2 %all-gather.6.cloned.1.call-start = ((), (), s32[]{:S(2)}) async-start(), calls=%async_computation.2 | async-start | bytes 2654208 | tf_op jit(solution)/shard_map/all_gather | solution.py:84
  20.9 304.6 %reduce-scatter.5.cloned.1.call-start = ((), (), s32[]{:S(2)}) async-start(), calls=%async_computation.6 | async-start | bytes 2359296 | tf_op jit(solution)/shard_map/reduce_scatter | solution.py:143
  22.8 20.6 %collective-permute-start = (bf16[288,512]{0,1:T(8,128)(2,1)}, bf16[288,512]{0,1:T(8,128)(2,1)S(1)}, u32[]{:S(2)}, u32[]{:S(2)}) collective-permute-start(bf16[288,512]{0,1:T(8,128)(2,1)} %copy.154), channel_id=1, source_target_pairs={{0,4},{4,8},{8,12},{12,16},{16,20},{20,24},{24,28},{28,0},{1,5},{5... | collective-permute-start | bytes 884744 | tf_op jit(solution)/shard_map/ppermute | solution.py:115
  43.4 66.2 %copy-start.4 = (bf16[288,512]{0,1:T(8,128)(2,1)}, bf16[288,512]{0,1:T(8,128)(2,1)S(1)}, u32[]{:S(2)}) copy-start(bf16[288,512]{0,1:T(8,128)(2,1)S(1)} %collective-permute-done) | copy-start | bytes 884740
  43.4 12.7 %collective-permute-start.1 = (bf16[288,512]{0,1:T(8,128)(2,1)S(1)}, bf16[288,512]{0,1:T(8,128)(2,1)S(1)}, u32[]{:S(2)}, u32[]{:S(2)}) collective-permute-start(bf16[288,512]{0,1:T(8,128)(2,1)S(1)} %collective-permute-done), channel_id=1, source_target_pairs={{0,4},{4,8},{8,12},{12,16},{16,20},{20,24},{24,28},{28,0},{1,5},{5... | collective-permute-start | bytes 884744 | tf_op jit(solution)/shard_map/ppermute | solution.py:115
  56.1 53.5 %copy-start.5 = (bf16[288,512]{0,1:T(8,128)(2,1)}, bf16[288,512]{0,1:T(8,128)(2,1)S(1)}, u32[]{:S(2)}) copy-start(bf16[288,512]{0,1:T(8,128)(2,1)S(1)} %collective-permute-done.1) | copy-start | bytes 884740
  56.1 19.8 %collective-permute-start.2 = (bf16[288,512]{0,1:T(8,128)(2,1)S(1)}, bf16[288,512]{0,1:T(8,128)(2,1)S(1)}, u32[]{:S(2)}, u32[]{:S(2)}) collective-permute-start(bf16[288,512]{0,1:T(8,128)(2,1)S(1)} %collective-permute-done.1), channel_id=1, source_target_pairs={{0,4},{4,8},{8,12},{12,16},{16,20},{20,24},{24,28},{28,0},{1,5},{5... | collective-permute-start | bytes 884744 | tf_op jit(solution)/shard_map/ppermute | solution.py:115
  76.0 33.6 %copy-start.6 = (bf16[288,512]{0,1:T(8,128)(2,1)}, bf16[288,512]{0,1:T(8,128)(2,1)S(1)}, u32[]{:S(2)}) copy-start(bf16[288,512]{0,1:T(8,128)(2,1)S(1)} %collective-permute-done.2) | copy-start | bytes 884740
  76.0 20.8 %collective-permute-start.3 = (bf16[288,512]{0,1:T(8,128)(2,1)S(1)}, bf16[288,512]{0,1:T(8,128)(2,1)S(1)}, u32[]{:S(2)}, u32[]{:S(2)}) collective-permute-start(bf16[288,512]{0,1:T(8,128)(2,1)S(1)} %collective-permute-done.2), channel_id=1, source_target_pairs={{0,4},{4,8},{8,12},{12,16},{16,20},{20,24},{24,28},{28,0},{1,5},{5... | collective-permute-start | bytes 884744 | tf_op jit(solution)/shard_map/ppermute | solution.py:115
  96.8 12.8 %copy-start.7 = (bf16[288,512]{0,1:T(8,128)(2,1)}, bf16[288,512]{0,1:T(8,128)(2,1)S(1)}, u32[]{:S(2)}) copy-start(bf16[288,512]{0,1:T(8,128)(2,1)S(1)} %collective-permute-done.3) | copy-start | bytes 884740
  96.8 12.8 %collective-permute-start.4 = (bf16[288,512]{0,1:T(8,128)(2,1)S(1)}, bf16[288,512]{0,1:T(8,128)(2,1)}, u32[]{:S(2)}, u32[]{:S(2)}) collective-permute-start(bf16[288,512]{0,1:T(8,128)(2,1)S(1)} %collective-permute-done.3), channel_id=1, source_target_pairs={{0,4},{4,8},{8,12},{12,16},{16,20},{20,24},{24,28},{28,0},{1,5},{5... | collective-permute-start | bytes 884744 | tf_op jit(solution)/shard_map/ppermute | solution.py:115
  109.6 18.6 %collective-permute-start.5 = (bf16[288,512]{0,1:T(8,128)(2,1)}, bf16[288,512]{0,1:T(8,128)(2,1)}, u32[]{:S(2)}, u32[]{:S(2)}) collective-permute-start(bf16[288,512]{0,1:T(8,128)(2,1)} %collective-permute-done.4), channel_id=1, source_target_pairs={{0,4},{4,8},{8,12},{12,16},{16,20},{20,24},{24,28},{28,0},{1,5},{5... | collective-permute-start | bytes 884744 | tf_op jit(solution)/shard_map/ppermute | solution.py:115
  111.2 0.7 copy-start.1
  128.2 70.2 %collective-permute-start.6 = (bf16[288,512]{0,1:T(8,128)(2,1)}, bf16[288,512]{0,1:T(8,128)(2,1)S(1)}, u32[]{:S(2)}, u32[]{:S(2)}) collective-permute-start(bf16[288,512]{0,1:T(8,128)(2,1)} %collective-permute-done.5), channel_id=1, source_target_pairs={{0,4},{4,8},{8,12},{12,16},{16,20},{20,24},{24,28},{28,0},{1,5},{5... | collective-permute-start | bytes 884744 | tf_op jit(solution)/shard_map/ppermute | solution.py:115
  198.4 9.5 %copy-start.8 = (bf16[288,512]{1,0:T(8,128)(2,1)S(1)}, bf16[288,512]{1,0:T(8,128)(2,1)}, u32[]{:S(2)}) copy-start(bf16[288,512]{1,0:T(8,128)(2,1)} %convolution_convert_fusion.2) | copy-start | bytes 884740
  198.4 9.5 %copy-start.9 = (bf16[288,512]{1,0:T(8,128)(2,1)S(1)}, bf16[288,512]{1,0:T(8,128)(2,1)}, u32[]{:S(2)}) copy-start(bf16[288,512]{1,0:T(8,128)(2,1)} %param.14) | copy-start | bytes 884740
  198.4 9.5 %copy-start.13 = (f32[4]{0:T(128)S(1)}, f32[4]{0:T(128)}, u32[]{:S(2)}) copy-start(f32[4]{0:T(128)} %param.21) | copy-start | bytes 52
  214.1 11.4 %copy-start.3 = (bf16[2304,512]{1,0:T(8,128)(2,1)S(1)}, bf16[2304,512]{1,0:T(8,128)(2,1)}, u32[]{:S(2)}) copy-start(bf16[2304,512]{1,0:T(8,128)(2,1)} %get-tuple-element.162) | copy-start | bytes 7077892 | tf_op jit(solution)/shard_map/cond
  259.2 3.2 copy-start.2
  259.2 3.2 copy-start.10
  259.2 3.2 copy-start.12
  259.2 93.9 %reduce-scatter.3.cloned.1.call-start = ((), (), s32[]{:S(2)}) async-start(), calls=%async_computation.5 | async-start | bytes 1474560 | tf_op jit(solution)/shard_map/reduce_scatter | solution.py:154
Sparse Core Ops, SparseCore 0:
  17.4 75.2 all-gather.9
  94.9 64.7 all-gather.7
  161.9 51.8 all-gather.5
  259.3 66.1 reduce-scatter.4
  328.5 24.5 reduce-scatter.2
